TPU v7x, 32 devices: a whole 2x2x4 slice. The times are simulated.
32 devices in a mesh: fs: 8 (over z, y), tp: 4 (over x, core).
Axes of the slice: x: 2, y: 2, z: 4, core: 2. Of those that a mesh axis runs over, the one named last changes fastest.
Arguments:
- hidden_states: bfloat16 [2048, 2048], P('tp', 'fs'), may hold values from -6 to 6
- norm_gain: float32 [2048], P('fs'), may hold values from 0.1 to 1.9
- gate_master: float32 [8, 2048, 7168], P(None, 'fs', 'tp'), may hold values from -0.125 to 0.125
- up_master: float32 [8, 2048, 7168], P(None, 'fs', 'tp'), may hold values from -0.125 to 0.125
- down_master: float32 [8, 2048, 7168], P(None, 'fs', 'tp'), may hold values from -0.0625 to 0.0625
- expert_ids: int32 [2048, 2], P('tp'), may hold values from 0 to 7, all different within a row; in each aligned block of 512 rows (0 to 511, 512 to 1023, ...) at most 256 rows name the same one
- route_logits: float32 [2048, 2], P('tp'), may hold values from -6 to 6
Outputs:
- gate_serve: bfloat16 [8, 2048, 7168], P('tp', None, 'fs')
- up_serve: bfloat16 [8, 2048, 7168], P('tp', None, 'fs')
- down_serve: bfloat16 [8, 2048, 7168], P('tp', None, 'fs')
- combined: bfloat16 [2048, 2048], P('tp', 'fs')
Inputs may be any that keep to these rules, and one draw needn't show every extreme that they name: `expert_ids`: the 2 entries of a row differ. Among the rows of one index of tp (aligned blocks of 512 rows) no expert is named more than 256 times, and in some blocks one expert is named exactly 256 times.
All inputs are finite; a program needn't handle non-finite values.
Results may differ from a plain program's by a relative error of at most 0.018.
Values may be sent and summed in bfloat16 or wider, within the bound.
A program may use at most 192 MiB of HBM per device.

v0:
```python
import jax
import jax.numpy as jnp
from jax import lax
from jax.sharding import PartitionSpec as P

EPSILON = 1e-06


def arrange(weights, groups, row_groups):
    experts, rows, columns = weights.shape
    blocks = row_groups // groups
    split = weights.reshape(experts // groups, groups, rows, blocks, columns // blocks)
    split = split.reshape(groups, experts // groups, rows, blocks, columns // blocks)
    return jnp.transpose(split, (0, 3, 1, 2, 4))


def regroup(moved, row_groups):
    return moved.reshape((row_groups,) + moved.shape[2:])


def settle(arrived):
    return arrived.reshape(arrived.shape[1], arrived.shape[2], arrived.shape[3])


def per_device(
    hidden_states, norm_gain, gate_master, up_master, down_master, expert_ids, route_logits
):
    groups = lax.axis_size("tp")
    row_groups = lax.axis_size("fs")
    experts = gate_master.shape[0]
    local_count = experts // groups
    tokens = hidden_states.shape[0]
    pieces = hidden_states.shape[1]
    model_width = pieces * row_groups
    capacity = tokens // 2
    scaled = norm_gain[None, :, None]
    gate_cast = arrange((scaled * gate_master).astype(jnp.bfloat16), groups, row_groups)
    up_cast = arrange((scaled * up_master).astype(jnp.bfloat16), groups, row_groups)
    down_cast = arrange(down_master.astype(jnp.bfloat16), groups, row_groups)
    sectioned = (
        lax.all_to_all(gate_cast, "tp", split_axis=0, concat_axis=0, tiled=True),
        lax.all_to_all(up_cast, "tp", split_axis=0, concat_axis=0, tiled=True),
        lax.all_to_all(down_cast, "tp", split_axis=0, concat_axis=0, tiled=True),
    )
    landed = (
        lax.all_to_all(
            regroup(sectioned[0], row_groups), "fs", split_axis=0, concat_axis=2, tiled=True
        ),
        lax.all_to_all(
            regroup(sectioned[1], row_groups), "fs", split_axis=0, concat_axis=2, tiled=True
        ),
        lax.all_to_all(
            regroup(sectioned[2], row_groups), "fs", split_axis=0, concat_axis=2, tiled=True
        ),
    )
    gate_serve, up_serve, down_serve = (settle(landed[0]), settle(landed[1]), settle(landed[2]))
    values = hidden_states.astype(jnp.float32)
    squares = lax.psum(jnp.sum(values * values, axis=1), "fs")
    normed = (values * lax.rsqrt(squares / model_width + EPSILON)[:, None]).astype(jnp.bfloat16)
    weights = jax.nn.softmax(route_logits, axis=1)
    chosen = (expert_ids[:, :, None] == jnp.arange(experts, dtype=jnp.int32)[None, None, :]).astype(
        jnp.int32
    )
    chosen = chosen.reshape(tokens * 2, experts)
    before = jnp.cumsum(chosen, axis=0) - chosen
    position = jnp.sum(before * chosen, axis=1)
    slot_ids = expert_ids.reshape(-1) * capacity + position
    slot_table = (
        slot_ids[None, :] == jnp.arange(experts * capacity, dtype=jnp.int32)[:, None]
    ).astype(jnp.bfloat16)
    dispatch = jnp.sum(slot_table.reshape(experts * capacity, tokens, 2), axis=2)
    whole_rows = lax.all_gather(normed, "fs", axis=1, tiled=True)
    packed = jnp.dot(dispatch, whole_rows, preferred_element_type=jnp.float32).astype(jnp.bfloat16)
    arrived = lax.all_to_all(
        packed.reshape(groups, local_count * capacity, model_width),
        "tp",
        split_axis=0,
        concat_axis=0,
        tiled=True,
    )
    arranged = arrived.reshape(groups, local_count, capacity, model_width)
    activations = []
    for expert_index in range(local_count):
        expert_rows = arranged[:, expert_index].reshape(groups * capacity, model_width)
        gate_pre = jnp.dot(
            expert_rows, gate_serve[expert_index], preferred_element_type=jnp.float32
        )
        up_pre = jnp.dot(expert_rows, up_serve[expert_index], preferred_element_type=jnp.float32)
        activations.append((jax.nn.silu(gate_pre) * up_pre).astype(jnp.bfloat16))
    stacked = jnp.stack(activations)
    summed = lax.psum_scatter(
        jnp.einsum("jdh,jsh->djs", down_serve, stacked, preferred_element_type=jnp.float32).astype(
            jnp.bfloat16
        ),
        "fs",
        scatter_dimension=0,
        tiled=True,
    )
    results = summed.reshape(pieces, local_count, groups, capacity)
    returned = lax.all_to_all(results, "tp", split_axis=2, concat_axis=1, tiled=True)
    flat_out = returned.reshape(pieces, experts * capacity)
    picked = jnp.take(flat_out, slot_ids, axis=1).reshape(pieces, tokens, 2).astype(jnp.float32)
    combined = jnp.sum(picked * weights[None, :, :], axis=2)
    return (gate_serve, up_serve, down_serve, jnp.transpose(combined).astype(jnp.bfloat16))


def solution(mesh):
    in_specs = (
        P("tp", "fs"),
        P("fs"),
        P(None, "fs", "tp"),
        P(None, "fs", "tp"),
        P(None, "fs", "tp"),
        P("tp", None),
        P("tp", None),
    )
    out_specs = (P("tp", None, "fs"), P("tp", None, "fs"), P("tp", None, "fs"), P("tp", "fs"))
    return jax.shard_map(
        per_device, mesh=mesh, in_specs=in_specs, out_specs=out_specs, check_vma=False
    )
```

profile of v0, /device:TPU:0, one launch (start us, length us, event | category | flops | bytes accessed | tf_op | source)
XLA Modules:
  0.0 1129.3 jit_solution(13469280187086125755)
XLA Ops:
  7.2 15.5 %multiply_convert_fusion = (bf16[8,256,1792]{2,1,0:T(8,128)(2,1)}, bf16[8,256,1792]{2,1,0:T(8,128)(2,1)}) fusion(f32[8,256,1792]{2,1,0:T(8,128)} %param.10, f32[256]{0:T(256)} %param.8, f32[8,256,1792]{2,1,0:T(8,128)} %param.9), kind=kLoop, calls=%fused_computation.1 | loop fusion | flops 14680064 | bytes 44041216 | tf_op jit(solution)/shard_map/convert_element_type | solution.py:38
  22.7 14.6 %reshape_reshape.9 = bf16[4,2,256,2,896]{4,3,2,1,0:T(2,128)(2,1)} reshape(bf16[8,256,1792]{2,1,0:T(8,128)(2,1)} %get-tuple-element.17) | data formatting | bytes 14680064 | tf_op jit(solution)/shard_map/reshape;reshape | solution.py:13
  37.3 7.5 copy.82
  50.3 14.6 %reshape_reshape.10 = bf16[4,2,256,2,896]{4,3,2,1,0:T(2,128)(2,1)} reshape(bf16[8,256,1792]{2,1,0:T(8,128)(2,1)} %get-tuple-element.16) | data formatting | bytes 14680064 | tf_op jit(solution)/shard_map/reshape;reshape | solution.py:13
  64.8 7.5 copy.81
  72.4 60.5 %all-to-all-done = bf16[4,2,2,256,896]{4,3,2,1,0:T(8,128)(2,1)} async-done(((bf16[4,2,2,256,896]{4,3,2,1,0:T(8,128)(2,1)}), bf16[4,2,2,256,896]{4,3,2,1,0:T(8,128)(2,1)}, u32[]{:S(2)}, u32[]{:S(2)}) %all-to-all-start) | async-done | bytes 7340064 | tf_op jit(solution)/shard_map/all_to_all | solution.py:41
  138.4 9.0 convert_element_type.55
  147.4 14.6 %reshape_reshape.11 = bf16[4,2,256,2,896]{4,3,2,1,0:T(2,128)(2,1)} reshape(bf16[8,256,1792]{2,1,0:T(8,128)(2,1)} %convert_element_type.55) | data formatting | bytes 14680064 | tf_op jit(solution)/shard_map/reshape;reshape | solution.py:13
  162.0 7.5 copy.80
  169.5 50.8 %all-to-all-done.2 = bf16[4,2,2,256,896]{4,3,2,1,0:T(8,128)(2,1)} async-done(((bf16[4,2,2,256,896]{4,3,2,1,0:T(8,128)(2,1)}), bf16[4,2,2,256,896]{4,3,2,1,0:T(8,128)(2,1)}, u32[]{:S(2)}, u32[]{:S(2)}) %all-to-all-start.2) | async-done | bytes 7340064 | tf_op jit(solution)/shard_map/all_to_all | solution.py:42
  226.1 22.6 %psum.7 = f32[512]{0:T(512)S(1)} all-reduce(f32[512]{0:T(512)S(1)} %fusion.7), channel_id=1, replica_groups=mesh['fs'=8,'tp'=4] {'fs'}, use_global_device_ids=true, to_apply=%region_5.6 | all-reduce | flops 512 | bytes 4096 | tf_op jit(solution)/shard_map/psum | solution.py:58
  255.4 42.4 %all-gather.2.cloned.1.call-done = bf16[512,2048]{1,0:T(8,128)(2,1)} async-done(((bf16[512,256]{1,0:T(8,128)(2,1)}), bf16[512,2048]{1,0:T(8,128)(2,1)}) %all-gather.2.cloned.1.call-update) | async-done | bytes 2097168 | tf_op jit(solution)/shard_map/all_gather | solution.py:72
  297.7 8.2 convolution_convert_fusion
  307.8 100.5 %all_to_all.80 = bf16[4,512,2048]{2,1,0:T(8,128)(2,1)} all-to-all(bf16[4,512,2048]{2,1,0:T(8,128)(2,1)} %bitcast.97), channel_id=1, replica_groups=mesh['fs'=8,'tp'=4] {'tp'}, dimensions={0} | all-to-all | bytes 16777216 | tf_op jit(solution)/shard_map/all_to_all | solution.py:74
  408.4 167.3 %all_to_all.81 = bf16[8,2,256,896]{3,2,1,0:T(8,128)(2,1)} all-to-all(bf16[8,2,256,896]{3,2,1,0:T(8,128)(2,1)} %bitcast.1), channel_id=1, replica_groups=mesh['fs'=8,'tp'=4] {'fs'}, dimensions={0} | all-to-all | bytes 14680064 | tf_op jit(solution)/shard_map/all_to_all | solution.py:46
  575.7 165.7 %all_to_all.82 = bf16[8,2,256,896]{3,2,1,0:T(8,128)(2,1)} all-to-all(bf16[8,2,256,896]{3,2,1,0:T(8,128)(2,1)} %bitcast.6), channel_id=1, replica_groups=mesh['fs'=8,'tp'=4] {'fs'}, dimensions={0} | all-to-all | bytes 14680064 | tf_op jit(solution)/shard_map/all_to_all | solution.py:49
  746.5 6.3 fusion.18
  756.7 9.6 copy.83
  770.0 7.0 fusion.20
  776.9 128.9 %all-to-all-done.5 = bf16[8,2,256,896]{3,2,1,0:T(8,128)(2,1)} async-done(((bf16[8,2,256,896]{3,2,1,0:T(8,128)(2,1)}), bf16[8,2,256,896]{3,2,1,0:T(8,128)(2,1)}, u32[]{:S(2)}, u32[]{:S(2)}) %all-to-all-start.5) | async-done | bytes 7340064 | tf_op jit(solution)/shard_map/all_to_all | solution.py:52
  910.1 9.0 fusion.21
  935.0 13.3 %convert_bitcast_fusion = bf16[2048,2,1024]{0,2,1:T(8,128)(2,1)} fusion(bf16[2,2048,896]{2,1,0:T(8,128)(2,1)S(1)} %bitcast.98, bf16[1,1024,896]{2,1,0:T(8,128)(2,1)} %fusion.6, bf16[1,1024,896]{2,1,0:T(8,128)(2,1)} %fusion.5), kind=kOutput, calls=%fused_computation.3 | convolution fusion | flops 7522222080 | bytes 19398656 | tf_op jit(solution)/shard_map/jdh,jsh->djs/dot_general | solution.py:92
  948.3 146.1 %reduce-scatter.2.cloned.1.call-done = bf16[256,2,1024]{0,2,1:T(8,128)(2,1)} async-done(((bf16[2048,2,1024]{0,2,1:T(8,128)(2,1)}), bf16[256,2,1024]{0,2,1:T(8,128)(2,1)}) %reduce-scatter.2.cloned.1.call-update) | async-done | bytes 1048592 | tf_op jit(solution)/shard_map/reduce_scatter | solution.py:91
  1101.0 13.6 %all-to-all-done.7 = bf16[256,2,4,256]{0,3,1,2:T(8,128)(2,1)S(1)} async-done(((bf16[256,2,4,256]{0,3,1,2:T(8,128)(2,1)}), bf16[256,2,4,256]{0,3,1,2:T(8,128)(2,1)S(1)}, u32[]{:S(2)}, u32[]{:S(2)}) %all-to-all-start.7) | async-done | bytes 1048608 | tf_op jit(solution)/shard_map/all_to_all | solution.py:100
  (66 shorter events, 72.4 us)
Async XLA Ops:
  44.8 88.1 %all-to-all-start = ((bf16[4,2,2,256,896]{4,3,2,1,0:T(8,128)(2,1)}), bf16[4,2,2,256,896]{4,3,2,1,0:T(8,128)(2,1)}, u32[]{:S(2)}, u32[]{:S(2)}) async-start(bf16[4,2,2,256,896]{4,3,2,1,0:T(8,128)(2,1)} %bitcast.95), calls=%async_computation | async-start | bytes 14680064 | tf_op jit(solution)/shard_map/all_to_all | solution.py:41
  132.9 87.4 %all-to-all-start.2 = ((bf16[4,2,2,256,896]{4,3,2,1,0:T(8,128)(2,1)}), bf16[4,2,2,256,896]{4,3,2,1,0:T(8,128)(2,1)}, u32[]{:S(2)}, u32[]{:S(2)}) async-start(bf16[4,2,2,256,896]{4,3,2,1,0:T(8,128)(2,1)} %bitcast.94), calls=%async_computation.2 | async-start | bytes 14680064 | tf_op jit(solution)/shard_map/all_to_all | solution.py:42
  220.3 5.6 copy-start.7
  220.3 29.3 %copy-start.8 = (s32[512,2]{0,1:T(2,128)S(1)}, s32[512,2]{0,1:T(2,128)}, u32[]{:S(2)}) copy-start(s32[512,2]{0,1:T(2,128)} %param.12) | copy-start | bytes 12292
  220.3 87.5 %all-to-all-start.4 = ((bf16[4,2,2,256,896]{4,3,2,1,0:T(8,128)(2,1)}), bf16[4,2,2,256,896]{4,3,2,1,0:T(8,128)(2,1)}, u32[]{:S(2)}, u32[]{:S(2)}) async-start(bf16[4,2,2,256,896]{4,3,2,1,0:T(8,128)(2,1)} %bitcast.93), calls=%async_computation.4 | async-start | bytes 14680064 | tf_op jit(solution)/shard_map/all_to_all | solution.py:43
  225.9 71.8 %all-gather.2.cloned.1.call-start = ((), (), s32[]{:S(2)}) async-start(), calls=%async_computation.9 | async-start | bytes 2359296 | tf_op jit(solution)/shard_map/all_gather | solution.py:72
  741.4 164.4 %all-to-all-start.5 = ((bf16[8,2,256,896]{3,2,1,0:T(8,128)(2,1)}), bf16[8,2,256,896]{3,2,1,0:T(8,128)(2,1)}, u32[]{:S(2)}, u32[]{:S(2)}) async-start(bf16[8,2,256,896]{3,2,1,0:T(8,128)(2,1)} %bitcast.11), calls=%async_computation.5 | async-start | bytes 14680064 | tf_op jit(solution)/shard_map/all_to_all | solution.py:52
  746.2 348.2 %reduce-scatter.2.cloned.1.call-start = ((), (), s32[]{:S(2)}) async-start(), calls=%async_computation.10 | async-start | bytes 9437184 | tf_op jit(solution)/shard_map/reduce_scatter | solution.py:91
  756.6 9.6 copy-start
  905.8 4.3 copy-start.3
  909.8 25.1 %copy-start.1 = (bf16[1,2,8,256,896]{4,3,2,1,0:T(8,128)(2,1)}, bf16[1,2,8,256,896]{4,3,2,1,0:T(8,128)(2,1)S(1)}, u32[]{:S(2)}) copy-start(bf16[1,2,8,256,896]{4,3,2,1,0:T(8,128)(2,1)S(1)} %copy.63) | copy-start | bytes 22020100
  910.1 9.0 copy-start.6
  919.1 5.8 copy-start.2
  919.1 5.7 copy-start.5
  924.8 4.5 copy-start.4
  948.3 152.5 %copy-start.9 = (f32[512,2]{0,1:T(2,128)S(1)}, f32[512,2]{0,1:T(2,128)}, u32[]{:S(2)}) copy-start(f32[512,2]{0,1:T(2,128)} %param.13) | copy-start | bytes 12292
  1096.7 17.9 %all-to-all-start.7 = ((bf16[256,2,4,256]{0,3,1,2:T(8,128)(2,1)}), bf16[256,2,4,256]{0,3,1,2:T(8,128)(2,1)S(1)}, u32[]{:S(2)}, u32[]{:S(2)}) async-start(bf16[256,2,4,256]{0,3,1,2:T(8,128)(2,1)} %copy.68), calls=%async_computation.8 | async-start | bytes 2097152 | tf_op jit(solution)/shard_map/all_to_all | solution.py:100
Sparse Core Ops, SparseCore 0:
  249.7 47.9 all-gather.1
  948.4 145.9 reduce-scatter.1
where the time goes:
time: 1130 us
  blocking collectives  456 us (40%)
  waiting for transfers between devices  444 us (39%)
  local copies, waits for them, and re-layouts  109 us (10%)
  matrix products  46.3 us (4%)
  other arithmetic  33.9 us (3%)
  starting transfers between devices  25.2 us (2%)
  between operations  14.3 us (1%)
    all_to_all x1, blocking collectives, per_device(): lax.all_to_all(regroup(sectioned[0], row_groups), 'fs', split_axis=0, con...  167 us
    all_to_all x1, blocking collectives, per_device(): lax.all_to_all(regroup(sectioned[1], row_groups), 'fs', split_axis=0, con...  166 us
    reduce_scatter x1, waiting for transfers between devices, per_device(): lax.psum_scatter(jnp.einsum('jdh,jsh->djs', down_serve, stacked, preferre...  146 us
    all_to_all x1, waiting for transfers between devices, per_device(): lax.all_to_all(regroup(sectioned[2], row_groups), 'fs', split_axis=0, con...  129 us
    all_to_all x1, blocking collectives, per_device(): lax.all_to_all(packed.reshape(groups, local_count * capacity, model_width...  101 us
    another operation x6, local copies, waits for them, and re-layouts, arrange(): split.reshape(groups, experts // groups, rows, blocks, columns // blocks)  66.3 us
    all_to_all x1, waiting for transfers between devices, per_device(): lax.all_to_all(gate_cast, 'tp', split_axis=0, concat_axis=0, tiled=True)  60.5 us
    all_to_all x1, waiting for transfers between devices, per_device(): lax.all_to_all(up_cast, 'tp', split_axis=0, concat_axis=0, tiled=True)  50.8 us
  transfers between devices with their start and end apart: 7, of which 7 were waited for; matrix products, arithmetic and copies ran while one was open for 9% of the time, Pallas kernels for 0%

commit v1 on v0

--- a/solution.py
+++ b/solution.py
@@ -1,9 +1,247 @@
+import functools
+
 import jax
 import jax.numpy as jnp
 from jax import lax
+from jax.experimental import pallas as pl
+from jax.experimental.pallas import tpu as pltpu
 from jax.sharding import PartitionSpec as P
 
 EPSILON = 1e-06
+SLOTS = 4
+MESH = pl.DeviceIdType.MESH
+
+
+def exchange_kernel(
+    groups, row_groups, expert, chunks, gain_ref, gate_ref, up_ref, down_ref, dep_ref,
+    gate_out, up_out, down_out, stage, cast, landed, load_sem,
+    send_a, recv_a, send_b, recv_b,
+):
+    me = lax.axis_index("tp")
+    row = lax.axis_index("fs")
+    blocks = row_groups // groups
+    masters = (gate_ref, up_ref, down_ref)
+    outs = (gate_out, up_out, down_out)
+    local_count = gate_ref.shape[0] // groups
+    rows, columns = gate_ref.shape[1:]
+    height = rows // chunks
+    width = columns // blocks
+
+    barrier = pltpu.get_barrier_semaphore()
+    for step in range(1, groups):
+        pl.semaphore_signal(
+            barrier, inc=1, device_id={"tp": lax.rem(me + step, groups)}, device_id_type=MESH
+        )
+    for step in range(1, row_groups):
+        pl.semaphore_signal(
+            barrier, inc=1, device_id={"fs": lax.rem(row + step, row_groups)}, device_id_type=MESH
+        )
+    order = [groups // 2] + [s for s in range(1, groups) if s != groups // 2] + [0]
+    units = [(w, c) for w in range(len(masters)) for c in range(chunks)]
+    jobs = [(u, s) for u in range(len(units)) for s in order]
+
+    def load(n):
+        u, s = jobs[n]
+        w, c = units[u]
+        number = lax.rem(me + s, groups) * local_count + expert
+        return pltpu.make_async_copy(
+            masters[w].at[number, pl.ds(c * height, height)],
+            stage.at[n % SLOTS],
+            load_sem.at[n % SLOTS],
+        )
+
+    for n in range(SLOTS):
+        load(n).start()
+    pl.semaphore_wait(barrier, groups - 1 + row_groups - 1)
+
+    def first(u, s):
+        return pltpu.make_async_remote_copy(
+            src_ref=cast.at[u, s],
+            dst_ref=landed.at[u, s - 1],
+            send_sem=send_a.at[u, s - 1],
+            recv_sem=recv_a.at[u, s - 1],
+            device_id={"tp": lax.rem(me + s, groups)},
+            device_id_type=MESH,
+        )
+
+    def place(u, source):
+        w, c = units[u]
+        start = pl.multiple_of(source * rows + c * height, height)
+        return outs[w].at[pl.ds(start, height)]
+
+    def second(u, s, b):
+        held = cast.at[u, 0] if s == 0 else landed.at[u, s - 1]
+        goal = lax.rem(me + groups - s, groups) * blocks + b
+        piece = held.at[:, pl.ds(b * width, width)]
+        remote = lambda: pltpu.make_async_remote_copy(
+            src_ref=piece,
+            dst_ref=place(u, row),
+            send_sem=send_b.at[u, s * blocks + b],
+            recv_sem=recv_b.at[u, row],
+            device_id={"fs": goal},
+            device_id_type=MESH,
+        )
+        local = lambda: pltpu.make_async_copy(piece, place(u, row), recv_b.at[u, row])
+        return goal, remote, local
+
+    def pass_on(u, s):
+        for b in range(blocks):
+            goal, remote, local = second(u, s, b)
+
+            @pl.when(goal != row)
+            def _():
+                remote().start()
+
+            @pl.when(goal == row)
+            def _():
+                local().start()
+
+    def forward(u):
+        for s in sorted(range(1, groups), key=lambda s: s == groups // 2):
+            first(u, s).wait_recv()
+            pass_on(u, s)
+
+    strip = 16
+    for n, (u, s) in enumerate(jobs):
+        w, c = units[u]
+        load(n).wait()
+        slot = n % SLOTS
+
+        def convert(i, carry):
+            at = pl.ds(pl.multiple_of(i * strip, strip), strip)
+            value = stage[slot, at, :]
+            if w < 2:
+                gain = gain_ref[pl.ds(pl.multiple_of(c * height + i * strip, strip), strip), :]
+                value = value * gain
+            cast[u, s, at, :] = value.astype(jnp.bfloat16)
+            return carry
+
+        lax.fori_loop(0, height // strip, convert, 0)
+        if n + SLOTS < len(jobs):
+            load(n + SLOTS).start()
+        if s == 0:
+            pass_on(u, 0)
+            if u >= 1:
+                forward(u - 1)
+        else:
+            first(u, s).start()
+    forward(len(units) - 1)
+    for u in range(len(units)):
+        for s in range(groups):
+            if s:
+                first(u, s).wait_send()
+            for b in range(blocks):
+                goal, remote, local = second(u, s, b)
+
+                @pl.when(goal != row)
+                def _():
+                    remote().wait_send()
+        for source in range(row_groups):
+            pltpu.make_async_copy(
+                cast.at[u, 0, :, pl.ds(0, width)], place(u, source), recv_b.at[u, source]
+            ).wait()
+
+
+def exchange(gain, gate, up, down, dep, expert, collective):
+    groups = lax.axis_size("tp")
+    row_groups = lax.axis_size("fs")
+    experts, rows, columns = gate.shape
+    blocks = row_groups // groups
+    width = columns // blocks
+    chunks = 2
+    units = 3 * chunks
+    height = rows // chunks
+    out = jax.ShapeDtypeStruct((rows * row_groups, width), jnp.bfloat16)
+    hbm = pl.BlockSpec(memory_space=pl.ANY)
+    sent = 3 * rows * columns * 2 * groups
+    return pl.pallas_call(
+        functools.partial(exchange_kernel, groups, row_groups, expert, chunks),
+        out_shape=(out, out, out),
+        in_specs=[pl.BlockSpec(memory_space=pltpu.VMEM), hbm, hbm, hbm, hbm],
+        out_specs=(hbm, hbm, hbm),
+        scratch_shapes=[
+            pltpu.VMEM((SLOTS, height, columns), jnp.float32),
+            pltpu.VMEM((units, groups, height, columns), jnp.bfloat16),
+            pltpu.VMEM((units, groups - 1, height, columns), jnp.bfloat16),
+            pltpu.SemaphoreType.DMA((SLOTS,)),
+            pltpu.SemaphoreType.DMA((units, groups - 1)),
+            pltpu.SemaphoreType.DMA((units, groups - 1)),
+            pltpu.SemaphoreType.DMA((units, row_groups)),
+            pltpu.SemaphoreType.DMA((units, row_groups)),
+        ],
+        compiler_params=pltpu.CompilerParams(
+            collective_id=collective, has_side_effects=True, vmem_limit_bytes=44 * 1024 * 1024
+        ),
+        cost_estimate=pl.CostEstimate(
+            flops=rows * columns, bytes_accessed=32 * sent, transcendentals=0
+        ),
+    )(gain, gate, up, down, dep)
+
+
+def fused_device(
+    hidden_states, norm_gain, gate_master, up_master, down_master, expert_ids, route_logits
+):
+    groups = lax.axis_size("tp")
+    row_groups = lax.axis_size("fs")
+    experts = gate_master.shape[0]
+    local_count = experts // groups
+    tokens, pieces = hidden_states.shape
+    model_width = pieces * row_groups
+    capacity = tokens // 2
+    me = lax.axis_index("tp")
+    gain = norm_gain[:, None]
+    raw = lax.all_gather(hidden_states, "fs", axis=1, tiled=True)
+    raw = lax.all_gather(raw, "tp", axis=0)
+    all_ids = lax.all_gather(expert_ids, "tp", axis=0)
+    earlier = (jnp.arange(tokens)[:, None] > jnp.arange(tokens)[None, :]).astype(jnp.bfloat16)
+    weights = jax.nn.softmax(route_logits, axis=1)
+    named = expert_ids[:, :, None] == jnp.arange(experts, dtype=jnp.int32)[None, None, :]
+    chosen = jnp.any(named, axis=1).astype(jnp.bfloat16)
+    before = jnp.dot(earlier, chosen, preferred_element_type=jnp.float32)
+    position = jnp.sum(jnp.where(named, before[:, None, :], 0.0), axis=2).astype(jnp.int32)
+    slot_ids = (expert_ids * capacity + position).reshape(-1)
+
+    dep = hidden_states
+    served = []
+    partials = []
+    for j in range(local_count):
+        gate, up, down = exchange(gain, gate_master, up_master, down_master, dep, j, 1 + j)
+        served.append((gate, up, down))
+        mine = jnp.any(all_ids == me * local_count + j, axis=2)
+        spot = jnp.einsum(
+            "ts,gs->gt", earlier, mine.astype(jnp.bfloat16), preferred_element_type=jnp.float32
+        ).astype(jnp.int32)
+        table = (
+            mine[:, None, :]
+            & (spot[:, None, :] == jnp.arange(capacity, dtype=jnp.int32)[None, :, None])
+        ).astype(jnp.bfloat16)
+        packed = jnp.einsum("gct,gtd->gcd", table, raw, preferred_element_type=jnp.float32)
+        packed = packed.reshape(groups * capacity, model_width)
+        mean = jnp.mean(packed * packed, axis=1, keepdims=True)
+        normed = (packed * lax.rsqrt(mean + EPSILON)).astype(jnp.bfloat16)
+        gate_pre = jnp.dot(normed, gate, preferred_element_type=jnp.float32)
+        up_pre = jnp.dot(normed, up, preferred_element_type=jnp.float32)
+        act = (jax.nn.silu(gate_pre) * up_pre).astype(jnp.bfloat16)
+        partial = jnp.einsum(
+            "dh,sh->ds", down, act, preferred_element_type=jnp.float32
+        ).astype(jnp.bfloat16)
+        partials.append(partial)
+        dep = partial
+    returned = []
+    for partial in partials:
+        summed = lax.psum_scatter(partial, "fs", scatter_dimension=0, tiled=True)
+        returned.append(
+            lax.all_to_all(
+                summed.reshape(pieces, groups, capacity), "tp", split_axis=1, concat_axis=1, tiled=True
+            )
+        )
+    flat_out = jnp.stack(returned, axis=2).reshape(pieces, experts * capacity)
+    picked = flat_out.at[:, slot_ids].get(mode="promise_in_bounds")
+    picked = picked.reshape(pieces, tokens, 2).astype(jnp.float32)
+    combined = jnp.sum(picked * weights[None, :, :], axis=2)
+    return tuple(jnp.stack([one[w] for one in served]) for w in range(3)) + (
+        jnp.transpose(combined).astype(jnp.bfloat16),
+    )
 
 
 def arrange(weights, groups, row_groups):
@@ -27,6 +265,11 @@
 ):
     groups = lax.axis_size("tp")
     row_groups = lax.axis_size("fs")
+    whole_tiles = gate_master.shape[2] // (row_groups // groups) % 128 == 0
+    if whole_tiles and gate_master.shape[1] % 256 == 0:
+        return fused_device(
+            hidden_states, norm_gain, gate_master, up_master, down_master, expert_ids, route_logits
+        )
     experts = gate_master.shape[0]
     local_count = experts // groups
     tokens = hidden_states.shape[0]

time: 1130 us -> 834 us (0.74)
  Pallas kernels: 0 us -> 498 us
  blocking collectives: 456 us -> 53.8 us
  waiting for transfers between devices: 444 us -> 134 us
  local copies, waits for them, and re-layouts: 109 us -> 17.7 us
  starting transfers between devices: 25.2 us -> 36.6 us
  other arithmetic: 33.9 us -> 22.5 us
    pallas_call x0 -> x2, Pallas kernels: none -> 498 us  [exchange(): pl.pallas_call(functools.partial(exchange_kernel, groups, row_groups, exp...]
    all_to_all x3 -> x0, blocking collectives: 434 us -> none  [the longest x1 167 us: per_device(): lax.all_to_all(regroup(sectioned[0], row_groups), 'fs', split_axis=0, con...]
    all_to_all x5 -> x2, waiting for transfers between devices: 256 us -> 1.62 us  [fused_device(): lax.all_to_all(summed.reshape(pieces, groups, capacity), 'tp', split_axis...]
    reduce_scatter x1 -> x2, waiting for transfers between devices: 146 us -> 76.3 us  [fused_device(): summed = lax.psum_scatter(partial, 'fs', scatter_dimension=0, tiled=True)]
    another operation x6 -> x1, local copies, waits for them, and re-layouts: 66.3 us -> 0.52 us  [fused_device(): flat_out = jnp.stack(returned, axis=2).reshape(pieces, experts * capacity)]
    all_gather x0 -> x1, blocking collectives: none -> 53.8 us  [fused_device(): all_ids = lax.all_gather(expert_ids, 'tp', axis=0)]
    convert_element_type x4 -> x3, other arithmetic: 25.4 us -> 1.08 us  [the longest x2 1.01 us: fused_device(): normed = (packed * lax.rsqrt(mean + EPSILON)).astype(jnp.bfloat16)]
    psum x1 -> x0, blocking collectives: 22.6 us -> none  [per_device(): squares = lax.psum(jnp.sum(values * values, axis=1), 'fs')]
  transfers between devices with their start and end apart: 7 -> 6, of which waited for: 7 -> 3; matrix products, arithmetic and copies ran while one was open for 9% -> 6% of each run, Pallas kernels for 0% -> 60%
where the time goes in v1:
time: 834 us
  Pallas kernels  498 us (60%)
  waiting for transfers between devices  134 us (16%)
  matrix products  57.5 us (7%)
  blocking collectives  53.8 us (6%)
  starting transfers between devices  36.6 us (4%)
  other arithmetic  22.5 us (3%)
  local copies, waits for them, and re-layouts  17.7 us (2%)
  between operations  14 us (2%)
    pallas_call x2, Pallas kernels, exchange(): pl.pallas_call(functools.partial(exchange_kernel, groups, row_groups, exp...  498 us
    reduce_scatter x2, waiting for transfers between devices, fused_device(): summed = lax.psum_scatter(partial, 'fs', scatter_dimension=0, tiled=True)  76.3 us
    all_gather x1, waiting for transfers between devices, fused_device(): raw = lax.all_gather(hidden_states, 'fs', axis=1, tiled=True)  55.2 us
    all_gather x1, blocking collectives, fused_device(): all_ids = lax.all_gather(expert_ids, 'tp', axis=0)  53.8 us
    all_to_all x2, starting transfers between devices, fused_device(): lax.all_to_all(summed.reshape(pieces, groups, capacity), 'tp', split_axis...  36.4 us
    dot_general x2, matrix products, fused_device(): jnp.einsum('dh,sh->ds', down, act, preferred_element_type=jnp.float32)  29.7 us
    another operation x2, other arithmetic, fused_device(): jnp.stack([one[w] for one in served])  17.6 us
  transfers between devices with their start and end apart: 6, of which 3 were waited for; matrix products, arithmetic and copies ran while one was open for 6% of the time, Pallas kernels for 60%

profile of v1, /device:TPU:0, one launch (start us, length us, event | category | flops | bytes accessed | tf_op | source)
XLA Modules:
  0.0 833.9 jit_solution(12522238898385166683)
XLA Ops:
  7.9 55.2 %all-gather.5.cloned.1.call-done = bf16[512,2048]{1,0:T(8,128)(2,1)} async-done(((bf16[512,256]{1,0:T(8,128)(2,1)}), bf16[512,2048]{1,0:T(8,128)(2,1)}) %all-gather.5.cloned.1.call-update) | async-done | bytes 2097168 | tf_op jit(solution)/shard_map/all_gather | solution.py:193
  64.0 0.9 copy-done.5
  65.0 221.1 %shard_map.102 = (bf16[2048,896]{1,0:T(8,128)(2,1)S(1)}, bf16[2048,896]{1,0:T(8,128)(2,1)S(1)}, bf16[2048,896]{1,0:T(8,128)(2,1)}) custom-call(f32[256,1]{1,0:T(8,128)S(1)} %copy.31.gain_ref, f32[8,256,1792]{2,1,0:T(8,128)} %gate_ref.3, f32[8,256,1792]{2,1,0:T(8,128)} %up_ref.3, f32[8,256,1792]{2,1,0:T(8,128)} %down_ref.3, bf16[512,256]{1,0:T(8,128)(2,1)S(1)} %copy-done.5), custom_call_target="tpu_custom_call" | custom-call | flops 458752 | bytes 352321536 | tf_op jit(solution)/shard_map/pallas_call | solution.py:157
  286.1 1.8 copy-done
  287.9 1.9 copy-done.2
  289.8 53.8 %all-gather = s32[2048,2]{0,1:T(2,128)S(1)} all-gather(s32[512,2]{0,1:T(2,128)S(1)} %copy-done.8), channel_id=2, replica_groups=mesh['fs'=8,'tp'=4] {'tp'}, dimensions={0}, use_global_device_ids=true | all-gather | bytes 20480 | tf_op jit(solution)/shard_map/all_gather | solution.py:195
  343.9 5.9 multiply_reduce_fusion.1
  350.4 2.9 copy-done.1
  353.3 6.3 fusion.16
  359.6 14.8 %convolution_convert_fusion.1.dep_ref = bf16[2048,1024]{1,0:T(8,128)(2,1)} fusion(bf16[2048,896]{1,0:T(8,128)(2,1)} %get-tuple-element.11, f32[1024,896]{1,0:T(8,128)} %fusion.16, bf16[1024,2048]{1,0:T(8,128)(2,1)} %copy-done.6, bf16[2048,896]{1,0:T(8,128)(2,1)} %copy-done.2), kind=kOutput, calls=%fused_computation.11 | convolution fusion | flops 7523794944 | bytes 19398656 | tf_op jit(solution)/shard_map/dh,sh->ds/dot_general | solution.py:225
  374.7 276.8 %shard_map.103 = (bf16[2048,896]{1,0:T(8,128)(2,1)S(1)}, bf16[2048,896]{1,0:T(8,128)(2,1)S(1)}, bf16[2048,896]{1,0:T(8,128)(2,1)}) custom-call(f32[256,1]{1,0:T(8,128)S(1)} %copy.31.gain_ref, f32[8,256,1792]{2,1,0:T(8,128)} %gate_ref.3, f32[8,256,1792]{2,1,0:T(8,128)} %up_ref.3, f32[8,256,1792]{2,1,0:T(8,128)} %down_ref.3, ...), custom_call_target="tpu_custom_call" | custom-call | flops 458752 | bytes 352321536 | tf_op jit(solution)/shard_map/pallas_call | solution.py:157
  651.5 8.6 %multiply_reduce_fusion = (f32[4,256]{1,0:T(4,128)S(1)}, f32[4,256,2048]{2,1,0:T(8,128)S(1)}) fusion(bf16[4,512,2048]{2,1,0:T(8,128)(2,1)} %bitcast.79, s32[4,512]{1,0:T(4,128)S(1)} %convolution_convert_fusion.2, pred[4,512]{1,0:T(4,128)(4,1)S(1)} %reshape.122), kind=kOutput, calls=%fused_computation.5 | convolution fusion | flops 2152725504 | bytes 16791552 | tf_op jit(solution)/shard_map/gct,gtd->gcd/dot_general | solution.py:218
  660.6 6.3 fusion.17
  667.0 14.9 %convolution_convert_fusion = bf16[2048,1024]{1,0:T(8,128)(2,1)} fusion(bf16[2048,896]{1,0:T(8,128)(2,1)} %get-tuple-element.15, f32[1024,896]{1,0:T(8,128)} %fusion.17, bf16[1024,2048]{1,0:T(8,128)(2,1)} %copy-done.7, bf16[2048,896]{1,0:T(8,128)(2,1)} %copy-done.4), kind=kOutput, calls=%fused_computation.10 | convolution fusion | flops 7523794944 | bytes 19398656 | tf_op jit(solution)/shard_map/dh,sh->ds/dot_general | solution.py:225
  682.9 1.9 copy.45
  684.7 32.8 %all-to-all-start = ((bf16[256,4,256]{2,0,1:T(8,128)(2,1)}), bf16[256,4,256]{2,0,1:T(8,128)(2,1)S(1)}, u32[]{:S(2)}, u32[]{:S(2)}) async-start(bf16[256,4,256]{2,0,1:T(8,128)(2,1)} %bitcast.73), calls=%async_computation.1 | async-start | bytes 1048576 | tf_op jit(solution)/shard_map/all_to_all | solution.py:234
  717.5 10.6 %pad_maximum_fusion = (bf16[2,2048,896]{2,1,0:T(8,128)(2,1)}, bf16[2,2048,896]{2,1,0:T(8,128)(2,1)}) fusion(bf16[1,2048,896]{2,1,0:T(8,128)(2,1)} %bitcast.76, bf16[1,2048,896]{2,1,0:T(8,128)(2,1)} %bitcast.74, bf16[1,2048,896]{2,1,0:T(8,128)(2,1)} %bitcast.77, bf16[1,2048,896]{2,1,0:T(8,128)(2,1)} %bitcast.75), kind=kLoop, calls=%fused_computation.7 | loop fusion | flops 7340032 | bytes 29360128 | tf_op jit(solution)/shard_map/stack | solution.py:242
  728.1 76.2 %reduce-scatter.5.cloned.1.call-done = bf16[256,1024]{1,0:T(8,128)(2,1)} async-done(((bf16[2048,1024]{1,0:T(8,128)(2,1)}), bf16[256,1024]{1,0:T(8,128)(2,1)}) %reduce-scatter.5.cloned.1.call-update) | async-done | bytes 524304 | tf_op jit(solution)/shard_map/reduce_scatter | solution.py:232
  804.4 1.9 copy.44
  806.3 3.7 all-to-all-start.1
  810.0 6.9 pad_maximum_fusion.2
  816.9 1.6 all-to-all-done.1
  819.1 3.9 gather_fusion
  823.8 3.6 multiply_reduce_fusion.2
  (55 shorter events, 5.5 us)
Async XLA Ops:
  7.2 56.0 %all-gather.5.cloned.1.call-start = ((), (), s32[]{:S(2)}) async-start(), calls=%async_computation.4 | async-start | bytes 2359296 | tf_op jit(solution)/shard_map/all_gather | solution.py:193
  7.9 336.0 %all-gather.7.cloned.1.call-start = ((), (), s32[]{:S(2)}) async-start(), calls=%async_computation.7 | async-start | bytes 10485760 | tf_op jit(solution)/shard_map/all_gather | solution.py:194
  63.1 619.7 %reduce-scatter.3.cloned.1.call-start = ((), (), s32[]{:S(2)}) async-start(), calls=%async_computation.5 | async-start | bytes 4718592 | tf_op jit(solution)/shard_map/reduce_scatter | solution.py:232
  64.0 1.0 copy-start.5
  65.0 224.8 %copy-start.8 = (s32[512,2]{0,1:T(2,128)S(1)}, s32[512,2]{0,1:T(2,128)}, u32[]{:S(2)}) copy-start(s32[512,2]{0,1:T(2,128)} %param.12) | copy-start | bytes 12292
  286.1 1.8 copy-start
  287.9 1.9 copy-start.2
  349.8 3.4 copy-start.1
  350.4 9.2 %copy-start.6 = (bf16[1024,2048]{1,0:T(8,128)(2,1)}, bf16[1024,2048]{1,0:T(8,128)(2,1)S(1)}, u32[]{:S(2)}) copy-start(bf16[1024,2048]{1,0:T(8,128)(2,1)S(1)} %fusion.1) | copy-start | bytes 12582916
  374.4 429.9 %reduce-scatter.5.cloned.1.call-start = ((), (), s32[]{:S(2)}) async-start(), calls=%async_computation.6 | async-start | bytes 4718592 | tf_op jit(solution)/shard_map/reduce_scatter | solution.py:232
  651.5 8.6 %copy-start.4 = (bf16[2048,896]{1,0:T(8,128)(2,1)}, bf16[2048,896]{1,0:T(8,128)(2,1)S(1)}, u32[]{:S(2)}) copy-start(bf16[2048,896]{1,0:T(8,128)(2,1)S(1)} %get-tuple-element.14) | copy-start | bytes 11010052
  651.5 9.1 %copy-start.3 = (bf16[2048,896]{1,0:T(8,128)(2,1)}, bf16[2048,896]{1,0:T(8,128)(2,1)S(1)}, u32[]{:S(2)}) copy-start(bf16[2048,896]{1,0:T(8,128)(2,1)S(1)} %get-tuple-element.13) | copy-start | bytes 11010052
  660.6 6.3 copy-start.7
  681.9 0.7 copy-start.9
  684.7 121.5 %all-to-all-start = ((bf16[256,4,256]{2,0,1:T(8,128)(2,1)}), bf16[256,4,256]{2,0,1:T(8,128)(2,1)S(1)}, u32[]{:S(2)}, u32[]{:S(2)}) async-start(bf16[256,4,256]{2,0,1:T(8,128)(2,1)} %bitcast.73), calls=%async_computation.1 | async-start | bytes 1048576 | tf_op jit(solution)/shard_map/all_to_all | solution.py:234
  806.3 12.3 %all-to-all-start.1 = ((bf16[256,4,256]{2,0,1:T(8,128)(2,1)}), bf16[256,4,256]{2,0,1:T(8,128)(2,1)S(1)}, u32[]{:S(2)}, u32[]{:S(2)}) async-start(bf16[256,4,256]{2,0,1:T(8,128)(2,1)} %bitcast.72), calls=%async_computation.3 | async-start | bytes 1048576 | tf_op jit(solution)/shard_map/all_to_all | solution.py:234
Sparse Core Ops, SparseCore 0:
  10.0 53.0 all-gather.4
  64.7 101.5 all-gather.6
  374.6 197.5 reduce-scatter.2
  682.0 122.2 reduce-scatter.4

commit v2 on v1

--- a/solution.py
+++ b/solution.py
@@ -178,6 +178,171 @@
     )(gain, gate, up, down, dep)
 
 
+def gather_sum_kernel(
+    groups, row_groups, partial_ref, early_ref, out_ref, early_out, own, pair, summed, far, total,
+    load_sem, send_a, recv_a, send_b, recv_b, send_c, recv_c, send_d, recv_d, early_sem,
+):
+    me = lax.axis_index("tp")
+    row = lax.axis_index("fs")
+    side = lax.rem(row, 2)
+    mate = row + 1 - 2 * side
+    stack = row_groups // 2
+    level = row // 2
+    pieces, slots = total.shape
+    capacity = slots // groups
+
+    barrier = pltpu.get_barrier_semaphore()
+    for step in range(1, groups):
+        pl.semaphore_signal(
+            barrier, inc=1, device_id={"tp": lax.rem(me + step, groups)}, device_id_type=MESH
+        )
+    for step in range(1, row_groups):
+        pl.semaphore_signal(
+            barrier, inc=1, device_id={"fs": lax.rem(row + step, row_groups)}, device_id_type=MESH
+        )
+    order = [stack // 2] + [k for k in range(1, stack) if k != stack // 2] + [0]
+
+    def rows_of(k, which):
+        goal = lax.rem(level + k, stack) * 2 + which
+        return partial_ref.at[pl.ds(pl.multiple_of(goal * pieces, pieces), pieces)]
+
+    def load(k):
+        return pltpu.make_async_copy(rows_of(k, side), own.at[k], load_sem.at[k])
+
+    def across(k):
+        return pltpu.make_async_remote_copy(
+            src_ref=rows_of(k, 1 - side),
+            dst_ref=pair.at[k],
+            send_sem=send_a.at[k],
+            recv_sem=recv_a.at[k],
+            device_id={"fs": mate},
+            device_id_type=MESH,
+        )
+
+    def along(k):
+        return pltpu.make_async_remote_copy(
+            src_ref=summed.at[k],
+            dst_ref=far.at[k],
+            send_sem=send_b.at[k],
+            recv_sem=recv_b.at[k],
+            device_id={"fs": lax.rem(level + k, stack) * 2 + side},
+            device_id_type=MESH,
+        )
+
+    def back(s):
+        goal = lax.rem(me + s, groups)
+        columns = pl.ds(pl.multiple_of(goal * capacity, capacity), capacity)
+        return pltpu.make_async_remote_copy(
+            src_ref=total.at[:, columns],
+            dst_ref=out_ref.at[me],
+            send_sem=send_c.at[s - 1],
+            recv_sem=recv_c.at[s - 1],
+            device_id={"tp": goal},
+            device_id_type=MESH,
+        )
+
+    def early_back(s):
+        goal = lax.rem(me + s, groups)
+        return pltpu.make_async_remote_copy(
+            src_ref=early_ref.at[goal],
+            dst_ref=early_out.at[me],
+            send_sem=send_d.at[s - 1],
+            recv_sem=recv_d.at[s - 1],
+            device_id={"tp": goal},
+            device_id_type=MESH,
+        )
+
+    for k in order:
+        load(k).start()
+    early_kept = pltpu.make_async_copy(early_ref.at[me], early_out.at[me], early_sem)
+    pl.semaphore_wait(barrier, groups - 1 + row_groups - 1)
+    for k in order:
+        across(k).start()
+    early_kept.start()
+    for s in range(1, groups):
+        early_back(s).start()
+    strip = 16
+    for k in order:
+        load(k).wait()
+        across(k).wait_recv()
+
+        def add(i, carry):
+            at = pl.ds(pl.multiple_of(i * strip, strip), strip)
+            both = own[k, at, :].astype(jnp.float32) + pair[k, at, :].astype(jnp.float32)
+            summed[k, at, :] = both.astype(jnp.bfloat16)
+            return carry
+
+        if k:
+            lax.fori_loop(0, pieces // strip, add, 0)
+            along(k).start()
+    for k in range(1, stack):
+        along(k).wait_recv()
+
+    def finish(i, carry):
+        at = pl.ds(pl.multiple_of(i * strip, strip), strip)
+        value = own[0, at, :].astype(jnp.float32) + pair[0, at, :].astype(jnp.float32)
+        for k in range(1, stack):
+            value = value + far[k, at, :].astype(jnp.float32)
+        total[at, :] = value.astype(jnp.bfloat16)
+        return carry
+
+    lax.fori_loop(0, pieces // strip, finish, 0)
+    for s in range(1, groups):
+        back(s).start()
+    columns = pl.ds(pl.multiple_of(me * capacity, capacity), capacity)
+    kept = pltpu.make_async_copy(total.at[:, columns], out_ref.at[me], load_sem.at[0])
+    kept.start()
+    kept.wait()
+    early_kept.wait()
+    for s in range(1, groups):
+        early_back(s).wait()
+        back(s).wait()
+    for k in range(stack):
+        across(k).wait_send()
+        if k:
+            along(k).wait_send()
+
+
+def gather_sum(partial, early, collective):
+    groups = lax.axis_size("tp")
+    row_groups = lax.axis_size("fs")
+    model_width, slots = partial.shape
+    pieces = model_width // row_groups
+    stack = row_groups // 2
+    capacity = slots // groups
+    block = pltpu.VMEM((stack, pieces, slots), jnp.bfloat16)
+    sent = model_width * slots * 2
+    return pl.pallas_call(
+        functools.partial(gather_sum_kernel, groups, row_groups),
+        out_shape=(
+            jax.ShapeDtypeStruct((groups, pieces, capacity), jnp.bfloat16),
+            jax.ShapeDtypeStruct(early.shape, jnp.bfloat16),
+        ),
+        in_specs=[pl.BlockSpec(memory_space=pl.ANY)] * 2,
+        out_specs=(pl.BlockSpec(memory_space=pl.ANY),) * 2,
+        scratch_shapes=[
+            block, block, block, block,
+            pltpu.VMEM((pieces, slots), jnp.bfloat16),
+            pltpu.SemaphoreType.DMA((stack,)),
+            pltpu.SemaphoreType.DMA((stack,)),
+            pltpu.SemaphoreType.DMA((stack,)),
+            pltpu.SemaphoreType.DMA((stack,)),
+            pltpu.SemaphoreType.DMA((stack,)),
+            pltpu.SemaphoreType.DMA((groups - 1,)),
+            pltpu.SemaphoreType.DMA((groups - 1,)),
+            pltpu.SemaphoreType.DMA((groups - 1,)),
+            pltpu.SemaphoreType.DMA((groups - 1,)),
+            pltpu.SemaphoreType.DMA,
+        ],
+        compiler_params=pltpu.CompilerParams(
+            collective_id=collective, has_side_effects=True, vmem_limit_bytes=20 * 1024 * 1024
+        ),
+        cost_estimate=pl.CostEstimate(
+            flops=sent, bytes_accessed=32 * sent, transcendentals=0
+        ),
+    )(partial, early)
+
+
 def fused_device(
     hidden_states, norm_gain, gate_master, up_master, down_master, expert_ids, route_logits
 ):
@@ -190,9 +355,14 @@
     capacity = tokens // 2
     me = lax.axis_index("tp")
     gain = norm_gain[:, None]
-    raw = lax.all_gather(hidden_states, "fs", axis=1, tiled=True)
-    raw = lax.all_gather(raw, "tp", axis=0)
-    all_ids = lax.all_gather(expert_ids, "tp", axis=0)
+    id_rows = expert_ids.size // pieces
+    sheet = expert_ids.astype(jnp.bfloat16).reshape(id_rows, pieces)
+    sheet = jnp.pad(sheet, ((0, -id_rows % 16), (0, 0)))
+    everything = lax.all_gather(jnp.concatenate([hidden_states, sheet]), ("fs", "tp"), axis=0)
+    everything = everything.reshape(row_groups, groups, -1, pieces)
+    all_ids = everything[0, :, tokens : tokens + id_rows].astype(jnp.int32)
+    all_ids = all_ids.reshape(groups, tokens, 2)
+    raw = jnp.transpose(everything[:, :, :tokens], (1, 2, 0, 3)).reshape(groups, tokens, model_width)
     earlier = (jnp.arange(tokens)[:, None] > jnp.arange(tokens)[None, :]).astype(jnp.bfloat16)
     weights = jax.nn.softmax(route_logits, axis=1)
     named = expert_ids[:, :, None] == jnp.arange(experts, dtype=jnp.int32)[None, None, :]
@@ -227,15 +397,14 @@
         ).astype(jnp.bfloat16)
         partials.append(partial)
         dep = partial
-    returned = []
-    for partial in partials:
-        summed = lax.psum_scatter(partial, "fs", scatter_dimension=0, tiled=True)
-        returned.append(
-            lax.all_to_all(
-                summed.reshape(pieces, groups, capacity), "tp", split_axis=1, concat_axis=1, tiled=True
-            )
-        )
-    flat_out = jnp.stack(returned, axis=2).reshape(pieces, experts * capacity)
+    early = [
+        lax.psum_scatter(partial, "fs", scatter_dimension=0, tiled=True)
+        for partial in partials[:-1]
+    ]
+    early = jnp.stack([jnp.swapaxes(one.reshape(pieces, groups, capacity), 0, 1) for one in early], 1)
+    last, early = gather_sum(partials[-1], early, 1 + local_count)
+    ordered = jnp.concatenate([early, last[:, None]], axis=1)
+    flat_out = jnp.moveaxis(ordered, 2, 0).reshape(pieces, experts * capacity)
     picked = flat_out.at[:, slot_ids].get(mode="promise_in_bounds")
     picked = picked.reshape(pieces, tokens, 2).astype(jnp.float32)
     combined = jnp.sum(picked * weights[None, :, :], axis=2)
@@ -266,7 +435,7 @@
     groups = lax.axis_size("tp")
     row_groups = lax.axis_size("fs")
     whole_tiles = gate_master.shape[2] // (row_groups // groups) % 128 == 0
-    if whole_tiles and gate_master.shape[1] % 256 == 0:
+    if whole_tiles and gate_master.shape[0] > groups and row_groups % 4 == 0 and expert_ids.size % hidden_states.shape[1] == 0:
         return fused_device(
             hidden_states, norm_gain, gate_master, up_master, down_master, expert_ids, route_logits
         )

time: 834 us -> 822 us (0.986)
  Pallas kernels: 498 us -> 677 us
  waiting for transfers between devices: 134 us -> 0.04 us
  blocking collectives: 53.8 us -> 0 us
  starting transfers between devices: 36.6 us -> 0.08 us
  local copies, waits for them, and re-layouts: 17.7 us -> 42.7 us
    pallas_call x0 -> x1, Pallas kernels: none -> 103 us  [gather_sum(): pl.pallas_call(functools.partial(gather_sum_kernel, groups, row_groups),...]
    reduce_scatter x2 -> x1, waiting for transfers between devices: 76.3 us -> 0.01 us  [fused_device(): lax.psum_scatter(partial, 'fs', scatter_dimension=0, tiled=True)]
    pallas_call x2, Pallas kernels: 498 us -> 573 us  [exchange(): pl.pallas_call(functools.partial(exchange_kernel, groups, row_groups, exp...]
    all_gather x2 -> x1, waiting for transfers between devices: 55.2 us -> 0.01 us  [fused_device(): lax.all_gather(jnp.concatenate([hidden_states, sheet]), ('fs', 'tp'), axi...]
    all_gather x1 -> x0, blocking collectives: 53.8 us -> none  [fused_device(): all_ids = lax.all_gather(expert_ids, 'tp', axis=0)]
    all_to_all x2 -> x0, starting transfers between devices: 36.4 us -> none  [fused_device(): lax.all_to_all(summed.reshape(pieces, groups, capacity), 'tp', split_axis...]
    unnamed x22 -> x31, local copies, waits for them, and re-layouts: 7.58 us -> 24.5 us
  transfers between devices with their start and end apart: 6 -> 2, of which waited for: 3 -> 0; matrix products, arithmetic and copies ran while one was open for 6% -> 6% of each run, Pallas kernels for 60% -> 70%
where the time goes in v2:
time: 822 us; the launch traced here: 821 us
  Pallas kernels  677 us (82%)
  matrix products  58.1 us (7%)
  local copies, waits for them, and re-layouts  42.7 us (5%)
  other arithmetic  28.9 us (4%)
  between operations  14.3 us (2%)
    pallas_call x2, Pallas kernels, exchange(): pl.pallas_call(functools.partial(exchange_kernel, groups, row_groups, exp...  573 us
    pallas_call x1, Pallas kernels, gather_sum(): pl.pallas_call(functools.partial(gather_sum_kernel, groups, row_groups),...  103 us
    dot_general x2, matrix products, fused_device(): jnp.einsum('dh,sh->ds', down, act, preferred_element_type=jnp.float32)  29.8 us
    unnamed x31, local copies, waits for them, and re-layouts  24.5 us
  transfers between devices with their start and end apart: 2, of which 0 were waited for; matrix products, arithmetic and copies ran while one was open for 6% of the time, Pallas kernels for 70%

profile of v2, /device:TPU:0, one launch (start us, length us, event | category | flops | bytes accessed | tf_op | source)
XLA Modules:
  0.0 820.8 jit_solution(15066995041462079423)
XLA Ops:
  10.0 1.7 fusion.14
  13.5 264.0 %shard_map.102 = (bf16[2048,896]{1,0:T(8,128)(2,1)S(1)}, bf16[2048,896]{1,0:T(8,128)(2,1)S(1)}, bf16[2048,896]{1,0:T(8,128)(2,1)}) custom-call(f32[256,1]{1,0:T(8,128)S(1)} %copy.26.gain_ref, f32[8,256,1792]{2,1,0:T(8,128)} %gate_ref.3, f32[8,256,1792]{2,1,0:T(8,128)} %up_ref.3, f32[8,256,1792]{2,1,0:T(8,128)} %down_ref.3, bf16[512,256]{1,0:T(8,128)(2,1)S(1)} %copy-done.10), custom_call_target="tpu_custom_call" | custom-call | flops 458752 | bytes 352321536 | tf_op jit(solution)/shard_map/pallas_call | solution.py:157
  277.5 1.8 copy-done.1
  279.4 1.9 copy-done.4
  281.3 7.5 slice_bitcast_fusion
  289.5 7.8 copy.35
  299.0 5.9 multiply_reduce_fusion.1
  305.5 2.9 copy-done.2
  308.4 6.3 fusion.18
  314.8 14.9 %convolution_convert_fusion.1.dep_ref = bf16[2048,1024]{1,0:T(8,128)(2,1)} fusion(bf16[2048,896]{1,0:T(8,128)(2,1)} %get-tuple-element.13, f32[1024,896]{1,0:T(8,128)} %fusion.18, bf16[1024,2048]{1,0:T(8,128)(2,1)} %copy-done.12, bf16[2048,896]{1,0:T(8,128)(2,1)} %copy-done.4), kind=kOutput, calls=%fused_computation.12 | convolution fusion | flops 7523794944 | bytes 19398656 | tf_op jit(solution)/shard_map/dh,sh->ds/dot_general | solution.py:395
  330.6 309.4 %shard_map.103 = (bf16[2048,896]{1,0:T(8,128)(2,1)S(1)}, bf16[2048,896]{1,0:T(8,128)(2,1)S(1)}, bf16[2048,896]{1,0:T(8,128)(2,1)}) custom-call(f32[256,1]{1,0:T(8,128)S(1)} %copy.26.gain_ref, f32[8,256,1792]{2,1,0:T(8,128)} %gate_ref.3, f32[8,256,1792]{2,1,0:T(8,128)} %up_ref.3, f32[8,256,1792]{2,1,0:T(8,128)} %down_ref.3, ...), custom_call_target="tpu_custom_call" | custom-call | flops 458752 | bytes 352321536 | tf_op jit(solution)/shard_map/pallas_call | solution.py:157
  640.0 1.8 copy-done.6
  641.8 1.8 copy-done.8
  645.4 9.1 %multiply_reduce_fusion = (f32[4,256]{1,0:T(4,128)S(1)}, f32[4,256,2048]{2,1,0:T(8,128)}) fusion(bf16[4,512,2048]{2,1,0:T(8,128)(2,1)} %bitcast.82, s32[4,512]{1,0:T(4,128)S(1)} %convolution_convert_fusion.2, pred[4,512]{1,0:T(4,128)(4,1)S(1)} %reduce_or.28), kind=kOutput, calls=%fused_computation.6 | convolution fusion | flops 2152725504 | bytes 16791552 | tf_op jit(solution)/shard_map/gct,gtd->gcd/dot_general | solution.py:388
  654.5 7.8 pad_maximum_fusion.2
  663.5 7.4 pad_maximum_fusion
  670.9 4.0 fusion
  674.9 2.0 copy-done.11
  676.9 6.3 fusion.19
  683.2 14.9 %convolution_convert_fusion.partial_ref = bf16[2048,1024]{1,0:T(8,128)(2,1)} fusion(bf16[2048,896]{1,0:T(8,128)(2,1)} %get-tuple-element.17, f32[1024,896]{1,0:T(8,128)} %fusion.19, bf16[1024,2048]{1,0:T(8,128)(2,1)} %copy-done.11, bf16[2048,896]{1,0:T(8,128)(2,1)} %copy-done.6), kind=kOutput, calls=%fused_computation.11 | convolution fusion | flops 7523794944 | bytes 19398656 | tf_op jit(solution)/shard_map/dh,sh->ds/dot_general | solution.py:395
  699.6 2.2 copy-done
  701.7 103.4 %shard_map.104 = (bf16[4,256,256]{2,1,0:T(8,128)(2,1)S(1)}, bf16[4,1,256,256]{3,2,1,0:T(8,128)(2,1)S(1)}) custom-call(bf16[2048,1024]{1,0:T(8,128)(2,1)S(1)} %copy-done, bf16[4,1,256,256]{3,2,1,0:T(8,128)(2,1)S(1)} %bitcast.79), custom_call_target="tpu_custom_call" | custom-call | flops 4194304 | bytes 134217728 | tf_op jit(solution)/shard_map/pallas_call | solution.py:315
  805.8 3.9 gather_fusion
  810.4 3.6 multiply_reduce_fusion.2
  (60 shorter events, 14.2 us)
Async XLA Ops:
  7.2 274.1 %all-gather.3.cloned.1.call-start = ((), (), s32[]{:S(2)}) async-start(), calls=%async_computation.2 | async-start | bytes 8921088 | tf_op jit(solution)/shard_map/all_gather | solution.py:361
  11.7 686.4 %reduce-scatter.2.cloned.1.call-start = ((), (), s32[]{:S(2)}) async-start(), calls=%async_computation.1 | async-start | bytes 4718592 | tf_op jit(solution)/shard_map/reduce_scatter | solution.py:401
  12.6 1.0 copy-start.10
  277.5 1.8 copy-start.1
  279.4 1.9 copy-start.4
  305.0 3.4 copy-start.2
  305.5 9.2 %copy-start.12 = (bf16[1024,2048]{1,0:T(8,128)(2,1)}, bf16[1024,2048]{1,0:T(8,128)(2,1)S(1)}, u32[]{:S(2)}) copy-start(bf16[1024,2048]{1,0:T(8,128)(2,1)S(1)} %fusion.1) | copy-start | bytes 12582916
  329.6 0.7 copy-start.13
  640.0 1.8 copy-start.6
  641.8 1.8 copy-start.8
  654.4 7.8 copy-start.3
  654.5 7.8 copy-start.5
  654.5 9.0 %copy-start.7 = (bf16[2048,896]{1,0:T(8,128)(2,1)S(1)}, bf16[2048,896]{1,0:T(8,128)(2,1)}, u32[]{:S(2)}) copy-start(bf16[2048,896]{1,0:T(8,128)(2,1)} %copy-done.6) | copy-start | bytes 11010052
  670.9 6.0 copy-start.9
  674.9 2.0 copy-start.11
  699.5 2.2 copy-start
Sparse Core Ops, SparseCore 0:
  11.8 174.8 all-gather.2
  329.8 231.7 reduce-scatter.1
